TPU v7x, 32 devices: a whole 2x2x4 slice. The times are simulated.
32 devices in a mesh: ep: 8 (over z, x), tp: 4 (over y, core).
Axes of the slice: x: 2, y: 2, z: 4, core: 2. Of those that a mesh axis runs over, the one named last changes fastest.
Arguments:
- queries: bfloat16 [4096, 2048], P('ep', 'tp'), may hold values from -5 to 5
- key_rows: bfloat16 [4096, 2048], P('ep', 'tp'), may hold values from -5 to 5
- values: bfloat16 [4096, 2048], P('ep', 'tp'), may hold values from -6 to 6
- forget_log: float32 [4096, 16], P(None, 'tp'), may hold values from -515 to 0, as said below
- out_weight: bfloat16 [2048, 4096], P(None, 'tp'), may hold values from -1 to 1
- expert_input: bfloat16 [1024, 4096], P(('ep', 'tp')), may hold values from -6 to 6
- norm_gain: float32 [4096], replicated, may hold values from 0.1 to 1.9
- route_ids: int32 [1024, 2], P('ep'), may hold values from 0 to 7, all different within a row; in each aligned block of 128 rows (0 to 127, 128 to 255, ...) at most 64 rows name the same one
- route_weights: float32 [1024, 2], P('ep'), may hold values from 0.2 to 1
- gate_weight: bfloat16 [8, 4096, 2048], P('ep', None, 'tp'), may hold values from -0.09375 to 0.09375
- up_weight: bfloat16 [8, 4096, 2048], P('ep', None, 'tp'), may hold values from -0.09375 to 0.09375
- down_weight: bfloat16 [8, 2048, 4096], P('ep', None, 'tp'), may hold values from -0.125 to 0.125
Outputs:
- mixer_out: bfloat16 [4096, 4096], P('ep', 'tp')
- expert_out: bfloat16 [1024, 4096], P('ep', 'tp')
Inputs may be any that keep to these rules, and one draw needn't show every extreme that they name: forget_log[t, h] is the sum of the log forget gates of head h at positions 0 to t of the one sequence; it never rises along positions. `route_ids`: each row names 2 different experts. In each aligned block of 128 rows (the rows of one index of ep) no expert is named by more than 64 rows, and some block reaches 64.
All inputs are finite; a program needn't handle non-finite values.
Results may differ from a plain program's by a relative error of at most 0.0071.
Values may be sent and summed in bfloat16 or wider, within the bound.
A program may use at most 64 MiB of HBM per device.

v0:
```python
import jax
import jax.numpy as jnp
from jax import lax
from jax.sharding import PartitionSpec as P

EPSILON = 1e-05


def slot_places(route_rows, experts, capacity):
    entries = route_rows.reshape(-1)
    matches = (entries[:, None] == jnp.arange(experts, dtype=jnp.int32)[None, :]).astype(jnp.int32)
    earlier = jnp.cumsum(matches, axis=0) - matches
    ranking = jnp.sum(earlier * matches, axis=1)
    return entries * capacity + ranking


def source_table(places, rows_count, chosen, total_slots):
    owners = jnp.arange(places.shape[0], dtype=jnp.int32) // chosen
    return jnp.full((total_slots,), rows_count, jnp.int32).at[places].set(owners)


def body(
    queries,
    key_rows,
    values,
    forget_log,
    out_weight,
    expert_input,
    norm_gain,
    route_ids,
    route_weights,
    gate_weight,
    up_weight,
    down_weight,
):
    row_count = queries.shape[0]
    heads_here = forget_log.shape[1]
    head_width = queries.shape[1] // heads_here
    own_start = lax.axis_index("ep") * row_count
    position_indices = own_start + jnp.arange(row_count, dtype=jnp.int32)
    query_heads = queries.reshape(row_count, heads_here, head_width)
    query_gate = lax.dynamic_slice_in_dim(forget_log, own_start, row_count, 0)
    score_scale = head_width ** (-0.5)

    def fold_shard(state_now, shard_item):
        first_row, key_shard, value_shard = shard_item

        def attend(state_in):
            row_max, row_total, weighted = state_in
            key_heads = key_shard.reshape(row_count, heads_here, head_width)
            value_heads = value_shard.reshape(row_count, heads_here, head_width)
            key_gate = lax.dynamic_slice_in_dim(forget_log, first_row, row_count, 0)
            scores = (
                jnp.einsum(
                    "qhd,khd->hqk", query_heads, key_heads, preferred_element_type=jnp.float32
                )
                * score_scale
            )
            scores = scores + query_gate.T[:, :, None] - key_gate.T[:, None, :]
            key_pos = first_row + jnp.arange(row_count, dtype=jnp.int32)
            scores = jnp.where(
                key_pos[None, None, :] <= position_indices[None, :, None], scores, -jnp.inf
            )
            newest = jnp.maximum(row_max, jnp.max(scores, axis=2))
            factor = jnp.exp(row_max - newest)
            weights_now = jnp.exp(scores - newest[:, :, None])
            row_total = row_total * factor + jnp.sum(weights_now, axis=2)
            weighted = weighted * factor[:, :, None] + jnp.einsum(
                "hqk,khd->hqd",
                weights_now.astype(jnp.bfloat16),
                value_heads,
                preferred_element_type=jnp.float32,
            )
            return (newest, row_total, weighted)

        return (
            lax.cond(first_row <= own_start, attend, lambda state_in: state_in, state_now),
            None,
        )

    initial = (
        jnp.full((heads_here, row_count), -jnp.inf, jnp.float32),
        jnp.zeros((heads_here, row_count), jnp.float32),
        jnp.zeros((heads_here, row_count, head_width), jnp.float32),
    )
    state_now = initial
    key_piece = lax.all_gather(key_rows, "ep", axis=0, tiled=True)
    value_piece = lax.all_gather(values, "ep", axis=0, tiled=True)
    shards = key_piece.shape[0] // row_count
    starts = row_count * jnp.arange(shards, dtype=jnp.int32)
    stacked = (
        starts,
        key_piece.reshape(shards, row_count, -1),
        value_piece.reshape(shards, row_count, -1),
    )
    state_now, _ = lax.scan(fold_shard, state_now, stacked)
    row_max, row_total, weighted = state_now
    attended = (
        (weighted / row_total[:, :, None])
        .transpose(1, 0, 2)
        .reshape(row_count, heads_here * head_width)
        .astype(jnp.bfloat16)
    )
    as_float = expert_input.astype(jnp.float32)
    center = jnp.mean(as_float, axis=1, keepdims=True)
    variance = jnp.mean(jnp.square(as_float - center), axis=1, keepdims=True)
    normed = ((as_float - center) * lax.rsqrt(variance + EPSILON) * norm_gain).astype(jnp.bfloat16)
    group_rows = lax.all_gather(normed, "tp", axis=0, tiled=True)
    block_rows = route_ids.shape[0]
    chosen = route_ids.shape[1]
    expert_local = gate_weight.shape[0]
    ep_count = lax.axis_size("ep")
    tp_count = lax.axis_size("tp")
    experts = expert_local * ep_count
    capacity = block_rows * chosen * 2 // experts
    places = slot_places(route_ids, experts, capacity)
    slot_table = source_table(places, block_rows, chosen, experts * capacity).reshape(
        ep_count, expert_local, capacity
    )
    share_size = capacity // tp_count
    part_table = lax.dynamic_slice_in_dim(
        slot_table, lax.axis_index("tp") * share_size, share_size, 2
    )
    outgoing = jnp.take(group_rows, part_table, axis=0, mode="fill", fill_value=0)
    arrived = lax.all_to_all(outgoing, "ep", split_axis=0, concat_axis=0, tiled=True)
    arrived_rows = lax.all_gather(arrived, "tp", axis=2, tiled=True)
    gate_part = jnp.einsum(
        "sxcd,xdf->sxcf", arrived_rows, gate_weight, preferred_element_type=jnp.float32
    )
    up_part = jnp.einsum(
        "sxcd,xdf->sxcf", arrived_rows, up_weight, preferred_element_type=jnp.float32
    )
    hidden = (jax.nn.silu(gate_part) * up_part).astype(jnp.bfloat16)
    slots_all = ep_count * expert_local * capacity
    flat_hidden = hidden.reshape(slots_all, hidden.shape[3])
    out_width = out_weight.shape[1]
    mixer_sum = jnp.dot(
        lax.all_gather(attended, "tp", axis=1, tiled=True),
        out_weight,
        preferred_element_type=jnp.float32,
    )
    part_rows = lax.all_gather(flat_hidden, "tp", axis=1, tiled=True)
    shaped = part_rows.reshape(ep_count, expert_local, capacity, part_rows.shape[1])
    product = jnp.einsum("sxcf,xfd->sxcd", shaped, down_weight, preferred_element_type=jnp.float32)
    expert_sum = product.reshape(slots_all, out_width)
    leaving = expert_sum.astype(jnp.bfloat16).reshape(ep_count, expert_local, capacity, out_width)
    returned = lax.all_to_all(leaving, "ep", split_axis=0, concat_axis=0, tiled=True)
    picked = jnp.take(returned.reshape(experts * capacity, out_width), places, axis=0).astype(
        jnp.float32
    )
    combined = jnp.sum(
        (picked * route_weights.reshape(-1)[:, None]).reshape(block_rows, chosen, out_width), axis=1
    )
    return (mixer_sum.astype(jnp.bfloat16), combined.astype(jnp.bfloat16))


def solution(mesh):
    placed = (
        P("ep", "tp"),
        P("ep", "tp"),
        P("ep", "tp"),
        P(None, "tp"),
        P(None, "tp"),
        P(("ep", "tp"), None),
        P(),
        P("ep", None),
        P("ep", None),
        P("ep", None, "tp"),
        P("ep", None, "tp"),
        P("ep", None, "tp"),
    )
    return jax.shard_map(
        body, mesh=mesh, in_specs=placed, out_specs=(P("ep", "tp"), P("ep", "tp")), check_vma=False
    )
```

profile of v0, /device:TPU:0, one launch (start us, length us, event | category | flops | bytes accessed | tf_op | source)
XLA Modules:
  0.0 390.9 jit_solution(14663094674887229282)
XLA Ops:
  9.5 1.8 fusion.51
  14.4 1.4 scatter_custom_fusion
  16.0 14.9 %all-gather.13.cloned.1.call-done = bf16[128,4096]{1,0:T(8,128)(2,1)} async-done(((bf16[32,4096]{1,0:T(8,128)(2,1)}), bf16[128,4096]{1,0:T(8,128)(2,1)}) %all-gather.13.cloned.1.call-update) | async-done | bytes 1048592 | tf_op jit(solution)/shard_map/all_gather | solution.py:108
  30.9 3.6 gather_fusion
  34.6 31.5 %all_to_all.10 = bf16[8,1,16,4096]{3,2,1,0:T(8,128)(2,1)} all-to-all(bf16[8,1,16,4096]{3,2,1,0:T(8,128)(2,1)S(1)} %broadcast_select_fusion), channel_id=1, replica_groups=mesh['ep'=8,'tp'=4] {'ep'}, dimensions={0} | all-to-all | bytes 2097152 | tf_op jit(solution)/shard_map/all_to_all | solution.py:125
  67.6 31.4 %all-gather.15.cloned.1.call-done = bf16[8,1,64,4096]{3,2,0,1:T(8,128)(2,1)} async-done(((bf16[8,1,16,4096]{3,2,0,1:T(8,128)(2,1)}), bf16[8,1,64,4096]{3,2,0,1:T(8,128)(2,1)}) %all-gather.15.cloned.1.call-update) | async-done | bytes 4194320 | tf_op jit(solution)/shard_map/all_gather | solution.py:126
  98.9 5.9 %fusion.27 = f32[8,1,64,512]{3,2,0,1:T(8,128)S(1)} fusion(bf16[1,4096,512]{2,1,0:T(8,128)(2,1)} %param.25, bf16[8,1,64,4096]{3,2,0,1:T(8,128)(2,1)} %all-gather.15.cloned.1.call-done), kind=kOutput, calls=%fused_computation.33 | convolution fusion | flops 2147483648 | bytes 9437184 | tf_op jit(solution)/shard_map/sxcd,xdf->sxcf/dot_general | solution.py:127
  104.9 3.2 fusion.42
  109.6 64.3 %all-gather.7.cloned.1.call-done = bf16[4096,512]{1,0:T(8,128)(2,1)} async-done(((bf16[512,512]{1,0:T(8,128)(2,1)}), bf16[4096,512]{1,0:T(8,128)(2,1)}) %all-gather.7.cloned.1.call-update) | async-done | bytes 4194320 | tf_op jit(solution)/shard_map/all_gather | solution.py:87
  173.9 6.5 %copy.58 = bf16[8,512,512]{1,2,0:T(8,128)(2,1)} copy(bf16[8,512,512]{2,1,0:T(8,128)(2,1)} %bitcast.117) | data formatting | bytes 8388608
  180.3 66.9 %all-gather.9.cloned.1.call-done = bf16[4096,512]{1,0:T(8,128)(2,1)} async-done(((bf16[512,512]{1,0:T(8,128)(2,1)}), bf16[4096,512]{1,0:T(8,128)(2,1)}) %all-gather.9.cloned.1.call-update) | async-done | bytes 4194320 | tf_op jit(solution)/shard_map/all_gather | solution.py:88
  247.2 6.5 %copy.60 = bf16[8,512,512]{1,2,0:T(8,128)(2,1)} copy(bf16[8,512,512]{2,1,0:T(8,128)(2,1)} %bitcast.118) | data formatting | bytes 8388608
  253.8 20.4 %while.16 = (s32[]{:T(128)}, f32[4,512]{1,0:T(4,128)S(1)}, f32[4,512]{1,0:T(4,128)S(1)}, f32[4,512,128]{2,1,0:T(8,128)S(1)}, s32[8]{0:T(128)S(1)}, /*index=5*/s3...) while((s32[]{:T(128)}, f32[4,512]{1,0:T(4,128)S(1)}, ...), condition=%wide.region_5.6_spmd.clone.clone, body=%wide.region_0.5_spmd.clone.clone.sunk | while | flops 555488256 | bytes 19607904 | solution.py:96
  255.1 10.0 %conditional.4 = ((f32[4,512]{1,0:T(4,128)S(1)}, f32[4,512]{1,0:T(4,128)S(1)}, f32[4,512,128]{2,1,0:T(8,128)S(1)})) conditional(s32[]{:T(128)} %convert_element_type.100, (f32[4,512]{1,0:T(4,128)S(1)}, f32[4,512]{1,0:T(4,128)S(1)}, f32[4,512,128]{2,1,0:T(8,128)S(1)}) %tuple.54, (s32[]{:T(128)}, s32[]{:T(128)}, bf16[8,512,512]{1,2,0:T(8,128)(2,1)}, ...), branch_computations={%region_1.1_spmd, %region_2.4_spmd} | conditional | flops 555488256 | bytes 19605586 | solution.py:77
  258.7 1.3 constant_dynamic-slice_fusion
  259.9 1.4 fusion.4
  261.4 1.4 fusion.3
  262.8 2.3 fusion.8
  275.5 6.1 %fusion.24 = bf16[8,1,64,1024]{3,2,1,0:T(8,128)(2,1)} fusion(bf16[8,64,2048]{2,1,0:T(8,128)(2,1)} %bitcast.129, bf16[1,2048,1024]{2,1,0:T(8,128)(2,1)} %param.27), kind=kOutput, calls=%fused_computation.32 | convolution fusion | flops 2148007936 | bytes 7340032 | tf_op jit(solution)/shard_map/sxcf,xfd->sxcd/dot_general | solution.py:144
  281.7 72.9 %all-to-all-start.1 = ((bf16[8,1,64,1024]{3,2,1,0:T(8,128)(2,1)}), bf16[8,1,64,1024]{3,2,1,0:T(8,128)(2,1)S(1)}, u32[]{:S(2)}, u32[]{:S(2)}) async-start(bf16[8,1,64,1024]{3,2,1,0:T(8,128)(2,1)} %fusion.24), calls=%async_computation.1 | async-start | bytes 2097152 | tf_op jit(solution)/shard_map/all_to_all | solution.py:147
  355.1 11.4 %all-gather.11.cloned.1.call-done = bf16[512,2048]{0,1:T(8,128)(2,1)} async-done(((bf16[512,512]{0,1:T(8,128)(2,1)}), bf16[512,2048]{0,1:T(8,128)(2,1)}) %all-gather.11.cloned.1.call-update) | async-done | bytes 2097168 | tf_op jit(solution)/shard_map/all_gather | solution.py:138
  366.5 6.1 %convolution_convert_fusion = bf16[512,1024]{1,0:T(8,128)(2,1)} fusion(bf16[512,2048]{0,1:T(8,128)(2,1)} %all-gather.11.cloned.1.call-done, bf16[2048,1024]{1,0:T(8,128)(2,1)} %param.20), kind=kOutput, calls=%fused_computation.31 | convolution fusion | flops 2148007936 | bytes 7340032 | tf_op jit(solution)/shard_map/dot_general | solution.py:137
  372.7 7.7 %all-to-all-done.1 = bf16[8,1,64,1024]{3,2,1,0:T(8,128)(2,1)S(1)} async-done(((bf16[8,1,64,1024]{3,2,1,0:T(8,128)(2,1)}), bf16[8,1,64,1024]{3,2,1,0:T(8,128)(2,1)S(1)}, u32[]{:S(2)}, u32[]{:S(2)}) %all-to-all-start.1) | async-done | bytes 1048608 | tf_op jit(solution)/shard_map/all_to_all | solution.py:147
  381.7 2.3 multiply_reduce_fusion
  (92 shorter events, 18.4 us)
Async XLA Ops:
  7.2 23.8 %all-gather.13.cloned.1.call-start = ((), (), s32[]{:S(2)}) async-start(), calls=%async_computation.5 | async-start | bytes 1310720 | tf_op jit(solution)/shard_map/all_gather | solution.py:108
  11.3 87.6 %all-gather.15.cloned.1.call-start = ((), (), s32[]{:S(2)}) async-start(), calls=%async_computation.6 | async-start | bytes 5242880 | tf_op jit(solution)/shard_map/all_gather | solution.py:126
  66.2 107.7 %all-gather.7.cloned.1.call-start = ((), (), s32[]{:S(2)}) async-start(), calls=%async_computation.2 | async-start | bytes 4718592 | tf_op jit(solution)/shard_map/all_gather | solution.py:87
  66.9 180.3 %all-gather.9.cloned.1.call-start = ((), (), s32[]{:S(2)}) async-start(), calls=%async_computation.3 | async-start | bytes 4718592 | tf_op jit(solution)/shard_map/all_gather | solution.py:88
  67.5 208.0 %all-gather.17.cloned.1.call-start = ((), (), s32[]{:S(2)}) async-start(), calls=%async_computation.7 | async-start | bytes 2621440 | tf_op jit(solution)/shard_map/all_gather | solution.py:142
  98.9 5.9 %copy-start.3 = (bf16[1,4096,512]{2,1,0:T(8,128)(2,1)S(1)}, bf16[1,4096,512]{2,1,0:T(8,128)(2,1)}, u32[]{:S(2)}) copy-start(bf16[1,4096,512]{2,1,0:T(8,128)(2,1)} %param.26) | copy-start | bytes 12582916
  98.9 5.9 %copy-start.4 = (bf16[8,1,64,4096]{3,2,0,1:T(8,128)(2,1)S(1)}, bf16[8,1,64,4096]{3,2,0,1:T(8,128)(2,1)}, u32[]{:S(2)}) copy-start(bf16[8,1,64,4096]{3,2,0,1:T(8,128)(2,1)} %all-gather.15.cloned.1.call-done) | copy-start | bytes 12582916
  104.9 3.5 copy-start
  108.1 258.4 %all-gather.11.cloned.1.call-start = ((), (), s32[]{:S(2)}) async-start(), calls=%async_computation.4 | async-start | bytes 2621440 | tf_op jit(solution)/shard_map/all_gather | solution.py:138
  275.5 79.3 %copy-start.1 = (s32[128,2]{0,1:T(2,128)S(1)}, s32[128,2]{0,1:T(2,128)}, u32[]{:S(2)}) copy-start(s32[128,2]{0,1:T(2,128)} %param.23) | copy-start | bytes 3076
  275.5 79.5 %copy-start.2 = (f32[128,2]{0,1:T(2,128)S(1)}, f32[128,2]{0,1:T(2,128)}, u32[]{:S(2)}) copy-start(f32[128,2]{0,1:T(2,128)} %param.24) | copy-start | bytes 3076
  281.7 98.6 %all-to-all-start.1 = ((bf16[8,1,64,1024]{3,2,1,0:T(8,128)(2,1)}), bf16[8,1,64,1024]{3,2,1,0:T(8,128)(2,1)S(1)}, u32[]{:S(2)}, u32[]{:S(2)}) async-start(bf16[8,1,64,1024]{3,2,1,0:T(8,128)(2,1)} %fusion.24), calls=%async_computation.1 | async-start | bytes 2097152 | tf_op jit(solution)/shard_map/all_to_all | solution.py:147
Sparse Core Ops, SparseCore 0:
  11.5 19.4 all-gather.12
  66.3 32.5 all-gather.14
  101.1 72.7 all-gather.6
  175.9 71.3 all-gather.8
  248.6 21.0 all-gather.16
  275.6 90.8 all-gather.10
where the time goes:
time: 392 us; the launch traced here: 391 us
  waiting for transfers between devices  198 us (51%)
  starting transfers between devices  73.3 us (19%)
  blocking collectives  31.5 us (8%)
  local copies, waits for them, and re-layouts  30 us (8%)
  matrix products  25.1 us (6%)
  between operations  14.3 us (4%)
  other arithmetic  11.3 us (3%)
  loops' own time  7.47 us (2%)
    all_to_all x1, starting transfers between devices, body(): lax.all_to_all(leaving, 'ep', split_axis=0, concat_axis=0, tiled=True)  72.9 us
    all_gather x1, waiting for transfers between devices, body(): value_piece = lax.all_gather(values, 'ep', axis=0, tiled=True)  66.9 us
    all_gather x1, waiting for transfers between devices, body(): key_piece = lax.all_gather(key_rows, 'ep', axis=0, tiled=True)  64.3 us
    all_to_all x1, blocking collectives, body(): lax.all_to_all(outgoing, 'ep', split_axis=0, concat_axis=0, tiled=True)  31.5 us
    all_gather x1, waiting for transfers between devices, body(): arrived_rows = lax.all_gather(arrived, 'tp', axis=2, tiled=True)  31.4 us
    all_gather x1, waiting for transfers between devices, body(): group_rows = lax.all_gather(normed, 'tp', axis=0, tiled=True)  14.9 us
    unnamed x16, local copies, waits for them, and re-layouts  14.4 us
    all_gather x1, waiting for transfers between devices, body(): lax.all_gather(attended, 'tp', axis=1, tiled=True)  11.4 us
  transfers between devices with their start and end apart: 7, of which 6 were waited for; matrix products, arithmetic and copies ran while one was open for 14% of the time, Pallas kernels for 0%

commit v1 on v0

--- a/solution.py
+++ b/solution.py
@@ -123,7 +123,12 @@
     )
     outgoing = jnp.take(group_rows, part_table, axis=0, mode="fill", fill_value=0)
     arrived = lax.all_to_all(outgoing, "ep", split_axis=0, concat_axis=0, tiled=True)
-    arrived_rows = lax.all_gather(arrived, "tp", axis=2, tiled=True)
+    ring = [arrived]
+    for hop in range(3):
+        ring.append(lax.ppermute(ring[-1], "tp", [(dev, (dev + 1) % 4) for dev in range(4)]))
+    arrived_rows = jnp.roll(
+        jnp.concatenate(ring[::-1], axis=2), (lax.axis_index("tp") + 1) * ring[0].shape[2], axis=2
+    )
     gate_part = jnp.einsum(
         "sxcd,xdf->sxcf", arrived_rows, gate_weight, preferred_element_type=jnp.float32
     )

time: 392 us -> 342 us (0.87)
  waiting for transfers between devices: 198 us -> 131 us
  blocking collectives: 31.5 us -> 48.3 us
  local copies, waits for them, and re-layouts: 30 us -> 34.3 us
    all_gather x1, waiting for transfers between devices: 64.3 us -> 0.01 us  [body(): key_piece = lax.all_gather(key_rows, 'ep', axis=0, tiled=True)]
    ppermute x0 -> x3, waiting for transfers between devices: none -> 42.7 us  [body(): lax.ppermute(ring[-1], 'tp', [(dev, (dev + 1) % 4) for dev in range(4)])]
    all_gather x1 -> x0, waiting for transfers between devices: 31.4 us -> none  [body(): arrived_rows = lax.all_gather(arrived, 'tp', axis=2, tiled=True)]
    all_to_all x1, blocking collectives: 31.5 us -> 48.3 us  [body(): lax.all_to_all(outgoing, 'ep', split_axis=0, concat_axis=0, tiled=True)]
    all_gather x1, waiting for transfers between devices: 66.9 us -> 54 us  [body(): value_piece = lax.all_gather(values, 'ep', axis=0, tiled=True)]
    unnamed x16 -> x23, local copies, waits for them, and re-layouts: 14.4 us -> 18.3 us
  transfers between devices with their start and end apart: 7 -> 9, of which waited for: 6 -> 7; matrix products, arithmetic and copies ran while one was open for 14% -> 17% of each run, Pallas kernels for 0% -> 0%
where the time goes in v1:
time: 342 us; the launch traced here: 340 us
  waiting for transfers between devices  131 us (38%)
  starting transfers between devices  73 us (21%)
  blocking collectives  48.3 us (14%)
  local copies, waits for them, and re-layouts  34.3 us (10%)
  matrix products  21.5 us (6%)
  between operations  14 us (4%)
  other arithmetic  11.3 us (3%)
  loops' own time  7.27 us (2%)
    all_to_all x1, starting transfers between devices, body(): lax.all_to_all(leaving, 'ep', split_axis=0, concat_axis=0, tiled=True)  72.6 us
    all_gather x1, waiting for transfers between devices, body(): value_piece = lax.all_gather(values, 'ep', axis=0, tiled=True)  54 us
    all_to_all x1, blocking collectives, body(): lax.all_to_all(outgoing, 'ep', split_axis=0, concat_axis=0, tiled=True)  48.3 us
    ppermute x3, waiting for transfers between devices, body(): lax.ppermute(ring[-1], 'tp', [(dev, (dev + 1) % 4) for dev in range(4)])  42.7 us
    unnamed x23, local copies, waits for them, and re-layouts  18.3 us
    all_gather x1, waiting for transfers between devices, body(): group_rows = lax.all_gather(normed, 'tp', axis=0, tiled=True)  14.1 us
    all_gather x1, waiting for transfers between devices, body(): lax.all_gather(attended, 'tp', axis=1, tiled=True)  11.4 us
    all_to_all x1, waiting for transfers between devices, body(): lax.all_to_all(leaving, 'ep', split_axis=0, concat_axis=0, tiled=True)  7.68 us
  transfers between devices with their start and end apart: 9, of which 7 were waited for; matrix products, arithmetic and copies ran while one was open for 17% of the time, Pallas kernels for 0%

profile of v1, /device:TPU:0, one launch (start us, length us, event | category | flops | bytes accessed | tf_op | source)
XLA Modules:
  0.0 340.5 jit_solution(4414645417046121677)
XLA Ops:
  9.5 1.8 fusion.43
  15.1 1.4 scatter_custom_fusion
  16.8 14.1 %all-gather.12.cloned.1.call-done = bf16[128,4096]{1,0:T(8,128)(2,1)} async-done(((bf16[32,4096]{1,0:T(8,128)(2,1)}), bf16[128,4096]{1,0:T(8,128)(2,1)}) %all-gather.12.cloned.1.call-update) | async-done | bytes 1048592 | tf_op jit(solution)/shard_map/all_gather | solution.py:108
  30.9 3.6 %gather_fusion = bf16[128,4096]{1,0:T(8,128)(2,1)S(1)} fusion(bf16[128,4096]{1,0:T(8,128)(2,1)} %all-gather.12.cloned.1.call-done, s32[1024]{0:T(1024)S(1)} %pad_clamp_fusion.1), kind=kCustom, calls=%fused_computation | custom fusion | bytes 2097664 | tf_op jit(solution)/shard_map/jit(_take)/gather | solution.py:124
  34.6 48.3 %all_to_all.10 = bf16[8,1,16,4096]{3,2,1,0:T(8,128)(2,1)S(1)} all-to-all(bf16[8,1,16,4096]{3,2,1,0:T(8,128)(2,1)S(1)} %broadcast_select_fusion), channel_id=1, replica_groups=mesh['ep'=8,'tp'=4] {'ep'}, dimensions={0} | all-to-all | bytes 2097152 | tf_op jit(solution)/shard_map/all_to_all | solution.py:125
  83.0 14.1 %collective-permute-done = bf16[8,1,16,4096]{3,2,1,0:T(8,128)(2,1)S(1)} collective-permute-done((bf16[8,1,16,4096]{3,2,1,0:T(8,128)(2,1)S(1)}, bf16[8,1,16,4096]{3,2,1,0:T(8,128)(2,1)S(1)}, u32[]{:S(2)}, u32[]{:S(2)}) %collective-permute-start) | collective-permute-done | bytes 1048608 | tf_op jit(solution)/shard_map/ppermute | solution.py:128
  97.1 14.2 %collective-permute-done.1 = bf16[8,1,16,4096]{3,2,1,0:T(8,128)(2,1)S(1)} collective-permute-done((bf16[8,1,16,4096]{3,2,1,0:T(8,128)(2,1)S(1)}, bf16[8,1,16,4096]{3,2,1,0:T(8,128)(2,1)S(1)}, u32[]{:S(2)}, u32[]{:S(2)}) %collective-permute-start.1) | collective-permute-done | bytes 1048608 | tf_op jit(solution)/shard_map/ppermute | solution.py:128
  111.4 14.3 %collective-permute-done.2 = bf16[8,1,16,4096]{3,2,1,0:T(8,128)(2,1)} collective-permute-done((bf16[8,1,16,4096]{3,2,1,0:T(8,128)(2,1)S(1)}, bf16[8,1,16,4096]{3,2,1,0:T(8,128)(2,1)}, u32[]{:S(2)}, u32[]{:S(2)}) %collective-permute-start.2) | collective-permute-done | bytes 1048608 | tf_op jit(solution)/shard_map/ppermute | solution.py:128
  127.3 1.4 constant_dynamic-update-slice_fusion.3
  129.8 2.3 fusion.29
  132.1 3.2 multiply_convert_fusion
  136.8 6.5 %copy.57 = bf16[8,512,512]{1,2,0:T(8,128)(2,1)} copy(bf16[8,512,512]{2,1,0:T(8,128)(2,1)} %bitcast.110) | data formatting | bytes 8388608
  143.3 54.0 %all-gather.8.cloned.1.call-done = bf16[4096,512]{1,0:T(8,128)(2,1)} async-done(((bf16[512,512]{1,0:T(8,128)(2,1)}), bf16[4096,512]{1,0:T(8,128)(2,1)}) %all-gather.8.cloned.1.call-update) | async-done | bytes 4194320 | tf_op jit(solution)/shard_map/all_gather | solution.py:88
  197.3 6.5 %copy.59 = bf16[8,512,512]{1,2,0:T(8,128)(2,1)} copy(bf16[8,512,512]{2,1,0:T(8,128)(2,1)} %bitcast.111) | data formatting | bytes 8388608
  203.9 20.4 %while.16 = (s32[]{:T(128)}, f32[4,512]{1,0:T(4,128)S(1)}, f32[4,512]{1,0:T(4,128)S(1)}, f32[4,512,128]{2,1,0:T(8,128)S(1)}, s32[8]{0:T(128)S(1)}, /*index=5*/s3...) while((s32[]{:T(128)}, f32[4,512]{1,0:T(4,128)S(1)}, ...), condition=%wide.region_5.6_spmd.clone.clone, body=%wide.region_0.5_spmd.clone.clone.sunk | while | flops 555488256 | bytes 19607896 | solution.py:96
  205.2 9.9 %conditional.4 = ((f32[4,512]{1,0:T(4,128)S(1)}, f32[4,512]{1,0:T(4,128)S(1)}, f32[4,512,128]{2,1,0:T(8,128)S(1)})) conditional(s32[]{:T(128)} %convert_element_type.100, (f32[4,512]{1,0:T(4,128)S(1)}, f32[4,512]{1,0:T(4,128)S(1)}, f32[4,512,128]{2,1,0:T(8,128)S(1)}) %tuple.54, (s32[]{:T(128)}, s32[]{:T(128)}, bf16[8,512,512]{1,2,0:T(8,128)(2,1)}, ...), branch_computations={%region_1.1_spmd, %region_2.4_spmd} | conditional | flops 555488256 | bytes 19605586 | solution.py:77
  210.0 1.4 fusion.4
  212.8 2.3 fusion.8
  225.7 6.1 %fusion.26 = bf16[8,1,64,1024]{3,2,1,0:T(8,128)(2,1)} fusion(bf16[8,64,2048]{2,1,0:T(8,128)(2,1)} %bitcast.121, bf16[1,2048,1024]{2,1,0:T(8,128)(2,1)} %param.27), kind=kOutput, calls=%fused_computation.34 | convolution fusion | flops 2148007936 | bytes 7340032 | tf_op jit(solution)/shard_map/sxcf,xfd->sxcd/dot_general | solution.py:149
  231.9 72.6 %all-to-all-start.1 = ((bf16[8,1,64,1024]{3,2,1,0:T(8,128)(2,1)}), bf16[8,1,64,1024]{3,2,1,0:T(8,128)(2,1)S(1)}, u32[]{:S(2)}, u32[]{:S(2)}) async-start(bf16[8,1,64,1024]{3,2,1,0:T(8,128)(2,1)} %fusion.26), calls=%async_computation.1 | async-start | bytes 2097152 | tf_op jit(solution)/shard_map/all_to_all | solution.py:152
  305.0 11.4 %all-gather.10.cloned.1.call-done = bf16[512,2048]{0,1:T(8,128)(2,1)} async-done(((bf16[512,512]{0,1:T(8,128)(2,1)}), bf16[512,2048]{0,1:T(8,128)(2,1)}) %all-gather.10.cloned.1.call-update) | async-done | bytes 2097168 | tf_op jit(solution)/shard_map/all_gather | solution.py:143
  316.4 6.1 %convolution_convert_fusion = bf16[512,1024]{1,0:T(8,128)(2,1)} fusion(bf16[512,2048]{0,1:T(8,128)(2,1)} %all-gather.10.cloned.1.call-done, bf16[2048,1024]{1,0:T(8,128)(2,1)} %param.20), kind=kOutput, calls=%fused_computation.33 | convolution fusion | flops 2148007936 | bytes 7340032 | tf_op jit(solution)/shard_map/dot_general | solution.py:142
  322.5 7.7 %all-to-all-done.1 = bf16[8,1,64,1024]{3,2,1,0:T(8,128)(2,1)S(1)} async-done(((bf16[8,1,64,1024]{3,2,1,0:T(8,128)(2,1)}), bf16[8,1,64,1024]{3,2,1,0:T(8,128)(2,1)S(1)}, u32[]{:S(2)}, u32[]{:S(2)}) %all-to-all-start.1) | async-done | bytes 1048608 | tf_op jit(solution)/shard_map/all_to_all | solution.py:152
  331.6 2.3 multiply_reduce_fusion
  (103 shorter events, 23.3 us)
Async XLA Ops:
  7.2 23.8 %all-gather.12.cloned.1.call-start = ((), (), s32[]{:S(2)}) async-start(), calls=%async_computation.5 | async-start | bytes 1310720 | tf_op jit(solution)/shard_map/all_gather | solution.py:108
  11.3 125.5 %all-gather.6.cloned.1.call-start = ((), (), s32[]{:S(2)}) async-start(), calls=%async_computation.2 | async-start | bytes 4718592 | tf_op jit(solution)/shard_map/all_gather | solution.py:87
  12.1 185.2 %all-gather.8.cloned.1.call-start = ((), (), s32[]{:S(2)}) async-start(), calls=%async_computation.3 | async-start | bytes 4718592 | tf_op jit(solution)/shard_map/all_gather | solution.py:88
  82.9 14.2 %collective-permute-start = (bf16[8,1,16,4096]{3,2,1,0:T(8,128)(2,1)S(1)}, bf16[8,1,16,4096]{3,2,1,0:T(8,128)(2,1)S(1)}, u32[]{:S(2)}, u32[]{:S(2)}) collective-permute-start(bf16[8,1,16,4096]{3,2,1,0:T(8,128)(2,1)S(1)} %all_to_all.10), channel_id=1, source_target_pairs={{0,1},{1,2},{2,3},{3,0},{4,5},{5,6},{6,7},{7,4},{8,9},{9,10},{10,1... | collective-permute-start | bytes 3145736 | tf_op jit(solution)/shard_map/ppermute | solution.py:128
  82.9 142.7 %all-gather.14.cloned.1.call-start = ((), (), s32[]{:S(2)}) async-start(), calls=%async_computation.6 | async-start | bytes 2621440 | tf_op jit(solution)/shard_map/all_gather | solution.py:147
  97.1 14.2 %collective-permute-start.1 = (bf16[8,1,16,4096]{3,2,1,0:T(8,128)(2,1)S(1)}, bf16[8,1,16,4096]{3,2,1,0:T(8,128)(2,1)S(1)}, u32[]{:S(2)}, u32[]{:S(2)}) collective-permute-start(bf16[8,1,16,4096]{3,2,1,0:T(8,128)(2,1)S(1)} %collective-permute-done), channel_id=1, source_target_pairs={{0,1},{1,2},{2,3},{3,0},{4,5},{5,6},{6,7},{7,4},{8,9},{9,10},{10,1... | collective-permute-start | bytes 3145736 | tf_op jit(solution)/shard_map/ppermute | solution.py:128
  111.4 14.3 %collective-permute-start.2 = (bf16[8,1,16,4096]{3,2,1,0:T(8,128)(2,1)S(1)}, bf16[8,1,16,4096]{3,2,1,0:T(8,128)(2,1)}, u32[]{:S(2)}, u32[]{:S(2)}) collective-permute-start(bf16[8,1,16,4096]{3,2,1,0:T(8,128)(2,1)S(1)} %collective-permute-done.1), channel_id=1, source_target_pairs={{0,1},{1,2},{2,3},{3,0},{4,5},{5,6},{6,7},{7,4},{8,9},{9,10},{10,1... | collective-permute-start | bytes 3145736 | tf_op jit(solution)/shard_map/ppermute | solution.py:128
  127.3 2.5 copy-start.3
  129.8 2.3 copy-start.4
  132.1 3.5 %copy-start = (bf16[512,512]{1,0:T(8,128)(2,1)S(1)}, bf16[512,512]{1,0:T(8,128)(2,1)}, u32[]{:S(2)}) copy-start(bf16[512,512]{1,0:T(8,128)(2,1)} %param.16) | copy-start | bytes 1572868
  135.4 181.0 %all-gather.10.cloned.1.call-start = ((), (), s32[]{:S(2)}) async-start(), calls=%async_computation.4 | async-start | bytes 2621440 | tf_op jit(solution)/shard_map/all_gather | solution.py:143
  225.7 79.0 %copy-start.1 = (s32[128,2]{0,1:T(2,128)S(1)}, s32[128,2]{0,1:T(2,128)}, u32[]{:S(2)}) copy-start(s32[128,2]{0,1:T(2,128)} %param.23) | copy-start | bytes 3076
  225.7 79.2 %copy-start.2 = (f32[128,2]{0,1:T(2,128)S(1)}, f32[128,2]{0,1:T(2,128)}, u32[]{:S(2)}) copy-start(f32[128,2]{0,1:T(2,128)} %param.24) | copy-start | bytes 3076
  231.9 98.4 %all-to-all-start.1 = ((bf16[8,1,64,1024]{3,2,1,0:T(8,128)(2,1)}), bf16[8,1,64,1024]{3,2,1,0:T(8,128)(2,1)S(1)}, u32[]{:S(2)}, u32[]{:S(2)}) async-start(bf16[8,1,64,1024]{3,2,1,0:T(8,128)(2,1)} %fusion.26), calls=%async_computation.1 | async-start | bytes 2097152 | tf_op jit(solution)/shard_map/all_to_all | solution.py:152
Sparse Core Ops, SparseCore 0:
  11.5 19.4 all-gather.11
  33.1 90.7 all-gather.5
  125.9 71.3 all-gather.7
  198.7 21.0 all-gather.13
  225.8 90.5 all-gather.9
